TPU v7x, 512 devices: a whole 4x8x8 slice. The times are simulated.
512 devices in a mesh: sp: 32 (over z, x), tp: 16 (over y, core).
Axes of the slice: x: 4, y: 8, z: 8, core: 2. Of those that a mesh axis runs over, the one named last changes fastest.
Arguments:
- pool_input: bfloat16 [1024, 12288], P('tp', 'sp'), may hold values from -6 to 6
- pool_gate: bfloat16 [1024, 12288], P('tp', 'sp'), may hold values from -6 to 6
- pool_mix: bfloat16 [4, 256, 256], replicated, may hold values from -0.375 to 0.375
- pool_scale: float32 [1024], replicated, may hold values from 0.1 to 1.9
- out_proj: bfloat16 [1024, 2048], P(None, 'tp'), may hold values from -0.375 to 0.375
- residual: bfloat16 [12288, 2048], P('sp', 'tp'), may hold values from -12 to 12
- norm_gain: float32 [2048], P('tp'), may hold values from 0.1 to 1.9
- routes: int32 [12288, 2], P('sp'), may hold values from 0 to 31, all different within a row; in each aligned block of 384 rows (0 to 383, 384 to 767, ...) at most 36 rows name the same one
- group_logits: float32 [12288, 4], P('sp'), may hold values from -4 to 4
- expert_scores: float32 [12288, 2], P('sp'), may hold values from -4 to 4
- w_gate: bfloat16 [32, 2048, 4096], P('sp', None, 'tp'), may hold values from -0.125 to 0.125
- w_up: bfloat16 [32, 2048, 4096], P('sp', None, 'tp'), may hold values from -0.125 to 0.125
- w_down: bfloat16 [32, 4096, 2048], P('sp', None, 'tp'), may hold values from -0.375 to 0.375
Outputs:
- layer_out: bfloat16 [12288, 2048], P('sp', 'tp')
Inputs may be any that keep to these rules, and one draw needn't show every extreme that they name: `routes`: among the rows of one device (aligned blocks of 384 rows) no expert is named by more than 36 rows, a bound that some block reaches; the 2 experts of a row differ.
All inputs are finite; a program needn't handle non-finite values.
Results may differ from a plain program's by a relative error of at most 0.01.
Values may be sent and summed in bfloat16 or wider, within the bound.
No kernel may reach another device: no remote copies, remote signals or barrier semaphores. Data moves between devices by JAX's collectives and lax.ppermute only.
A program may use at most 64 MiB of HBM per device.

v0:
```python
import jax
import jax.numpy as jnp
from jax import lax
from jax.sharding import PartitionSpec as P

D = 2048
POOL_GROUP = 256
TOP = 2
reach_back = 15
epsilon = 1e-06


def from_behind(value, axis, steps):
    count = lax.axis_size(axis)
    initial, last = (max(0, -steps), min(count, count - steps))
    return lax.ppermute(value, axis, [(source, source + steps) for source in range(initial, last)])


def in_one_piece(arrays, axis, dim, along):
    ends, at = ([], 0)
    for a in arrays[:-1]:
        at += a.shape[along]
        ends.append(at)
    both = jnp.concatenate(arrays, axis=along)
    return tuple(jnp.split(lax.all_gather(both, axis, axis=dim, tiled=True), ends, axis=along))


def from_everyone(value, axis):
    count = lax.axis_size(axis)
    return lax.all_to_all(
        jnp.broadcast_to(value[None], (count, *value.shape)), axis, 0, 0, tiled=True
    )


def over_copies(value, axis):
    return from_everyone(value, axis).sum(axis=0)


def window_terms(extended, first_channel, first_position, group_width):
    length = extended.shape[1] - reach_back
    layered = extended
    stride = 1
    partial_sums = []
    for _ in range(4):
        layered = layered[:, stride:] + layered[:, :-stride]
        stride = stride * 2
        partial_sums.append(layered[:, layered.shape[1] - length :])
    channel = first_channel + jnp.arange(extended.shape[0], dtype=jnp.int32)
    scale_index = channel // group_width
    chosen = partial_sums[3]
    for octave in range(3):
        chosen = jnp.where((scale_index == octave)[:, None], partial_sums[octave], chosen)
    window = (2 ** (scale_index + 1)).astype(jnp.float32)
    positions = (first_position + jnp.arange(length, dtype=jnp.int32) + 1).astype(jnp.float32)
    counted = jnp.minimum(positions[None, :], window[:, None])
    return chosen / counted - extended[:, reach_back:]


def slot_table(row_block, experts, capacity):
    flattened = row_block.reshape(-1)
    onehot = (flattened[:, None] == jnp.arange(experts, dtype=jnp.int32)[None, :]).astype(jnp.int32)
    before = jnp.cumsum(onehot, axis=0) - onehot
    ranked = jnp.sum(before * onehot, axis=1)
    return flattened * capacity + ranked


def route_weights(routes, group_logits, expert_scores, per_group):
    raised = jnp.exp(group_logits)
    group_prob = raised / jnp.sum(raised, axis=1, keepdims=True)
    owning_group = routes // per_group
    groups_iota = jnp.arange(group_logits.shape[1], dtype=jnp.int32)
    picked = jnp.sum(
        jnp.where(
            owning_group[:, :, None] == groups_iota[None, None, :], group_prob[:, None, :], 0.0
        ),
        axis=2,
    )
    lifted = jnp.exp(expert_scores)
    return picked * lifted / jnp.sum(lifted, axis=1, keepdims=True)


def per_device(
    pool_input,
    pool_gate,
    pool_mix,
    pool_scale,
    out_proj,
    residual,
    norm_gain,
    routes,
    group_logits,
    expert_scores,
    w_gate,
    w_up,
    w_down,
):
    channels, length = pool_input.shape
    edge_rows = from_behind(pool_input[:, length - reach_back :], "sp", 1)
    extended = jnp.concatenate([edge_rows, pool_input], axis=1).astype(jnp.float32)
    first_channel = lax.axis_index("tp") * channels
    first_position = lax.axis_index("sp") * length
    pooled = window_terms(extended, first_channel, first_position, POOL_GROUP).astype(jnp.bfloat16)
    gathered, gate_rows = in_one_piece((pooled, pool_gate), "tp", 0, 1)
    scales = pool_mix.shape[0]
    mixed_rows = jnp.einsum(
        "gct,gcd->tgd",
        gathered.reshape(scales, POOL_GROUP, length),
        pool_mix,
        preferred_element_type=jnp.float32,
    ).reshape(length, scales * POOL_GROUP)
    branch = (
        jax.nn.sigmoid(gate_rows.T.astype(jnp.float32)) * mixed_rows * pool_scale[None, :]
    ).astype(jnp.bfloat16)
    hidden_state = (
        residual.astype(jnp.float32) + jnp.dot(branch, out_proj, preferred_element_type=jnp.float32)
    ).astype(jnp.bfloat16)
    state_float = hidden_state.astype(jnp.float32)
    squares = over_copies(jnp.sum(state_float * state_float, axis=1), "tp")
    normed = (state_float * lax.rsqrt(squares / D + epsilon)[:, None] * norm_gain[None, :]).astype(
        jnp.bfloat16
    )
    experts = lax.axis_size("sp") * w_gate.shape[0]
    weights = route_weights(routes, group_logits, expert_scores, experts // group_logits.shape[1])
    capacity = 3 * TOP * length // (2 * experts)
    destination = slot_table(routes, experts, capacity)
    token_index = jnp.arange(length * TOP, dtype=jnp.int32) // TOP
    sources = jnp.full((experts * capacity,), length, jnp.int32).at[destination].set(token_index)
    padded = jnp.concatenate([normed, jnp.zeros((1, normed.shape[1]), jnp.bfloat16)], axis=0)
    arrived = lax.all_to_all(padded[sources], "sp", split_axis=0, concat_axis=0, tiled=True)
    portion = lax.all_gather(arrived, "tp", axis=1, tiled=True)
    rows_gate = w_gate[0]
    rows_up = w_up[0]
    gate_term = jnp.dot(portion, rows_gate, preferred_element_type=jnp.float32)
    up_term = jnp.dot(portion, rows_up, preferred_element_type=jnp.float32)
    activated = (jax.nn.silu(gate_term) * up_term).astype(jnp.bfloat16)
    rows_down = w_down[0]
    result = jnp.dot(
        lax.all_gather(activated, "tp", axis=1, tiled=True),
        rows_down,
        preferred_element_type=jnp.float32,
    ).astype(jnp.bfloat16)
    returned = lax.all_to_all(result, "sp", split_axis=0, concat_axis=0, tiled=True)
    picked = returned[destination].astype(jnp.float32).reshape(length, TOP, returned.shape[1])
    combined = jnp.sum(weights[:, :, None] * picked, axis=1)
    return (state_float + combined).astype(jnp.bfloat16)


def solution(mesh):
    placed = (
        P("tp", "sp"),
        P("tp", "sp"),
        P(),
        P(),
        P(None, "tp"),
        P("sp", "tp"),
        P("tp"),
        P("sp", None),
        P("sp", None),
        P("sp", None),
        P("sp", None, "tp"),
        P("sp", None, "tp"),
        P("sp", None, "tp"),
    )
    return jax.shard_map(
        per_device, mesh=mesh, in_specs=placed, out_specs=P("sp", "tp"), check_vma=False
    )
```

profile of v0, /device:TPU:16, one launch (start us, length us, event | category | flops | bytes accessed | tf_op | source)
XLA Modules:
  0.0 268.7 jit_solution(10977367310961019468)
XLA Ops:
  6.5 0.9 slice.43
  7.4 3.4 %collective-permute-start = (bf16[64,15]{1,0:T(8,128)(2,1)S(1)}, bf16[64,15]{1,0:T(8,128)(2,1)S(1)}, u32[]{:S(2)}, u32[]{:S(2)}) collective-permute-start(bf16[64,15]{1,0:T(8,128)(2,1)S(1)} %slice.43), channel_id=1, source_target_pairs={{0,16},{16,32},{32,48},{48,64},{64,80},{80,96},{96,112},{112,128},... | collective-permute-start | bytes 5768 | tf_op jit(solution)/shard_map/ppermute | solution.py:16
  10.9 1.3 collective-permute-done
  12.2 0.9 maximum_convert_fusion
  13.1 0.1 slice_add_fusion.2
  13.2 0.1 slice_add_fusion.1
  13.3 0.1 slice_add_fusion
  13.5 0.2 fusion.13
  13.7 0.7 pad_maximum_fusion
  14.4 0.1 copy.36
  14.5 0.1 eq.69
  14.7 0.1 eq.65
  14.8 1.7 reduce-window.6
  16.6 0.3 slice_reduce_fusion
  16.9 0.1 copy.35
  17.0 0.2 mul.134
  17.2 0.1 fusion.12
  17.3 3.4 %scatter_custom_fusion = s32[1152]{0:T(1024)S(1)} fusion(s32[768]{0:T(1024)S(1)} %fusion.24, s32[768]{0:T(1024)S(1)} %add_select_fusion, s32[]{:T(128)} %constant.90.clone.1), kind=kCustom, calls=%fused_computation.60 | custom fusion | bytes 4612 | tf_op jit(solution)/shard_map/scatter | solution.py:127
  20.7 39.9 %all-gather.4.cloned.1.call-done = bf16[1024,768]{1,0:T(8,128)(2,1)} async-done(((bf16[64,768]{1,0:T(8,128)(2,1)}), bf16[1024,768]{1,0:T(8,128)(2,1)}) %all-gather.4.cloned.1.call-update) | async-done | bytes 1572880 | tf_op jit(solution)/shard_map/all_gather | solution.py:25
  60.7 1.6 slice-done
  62.3 0.5 fusion.26
  62.8 0.4 fusion.2
  63.3 0.5 copy-done.3
  63.7 0.0 copy-done.4
  63.8 0.5 multiply_reduce_fusion
  64.3 0.6 broadcast_in_dim.69
  64.9 6.4 %all-to-all-start = ((f32[16,1,384]{2,1,0:T(1,128)}), f32[16,1,384]{2,1,0:T(1,128)S(1)}, u32[]{:S(2)}, u32[]{:S(2)}) async-start(f32[16,1,384]{2,1,0:T(1,128)} %broadcast_in_dim.69), calls=%async_computation | async-start | bytes 49152 | tf_op jit(solution)/shard_map/all_to_all | solution.py:30
  71.3 0.0 all-gather.6.cloned.1.call-start
  71.3 5.4 %all-to-all-done = f32[16,1,384]{2,1,0:T(1,128)S(1)} async-done(((f32[16,1,384]{2,1,0:T(1,128)}), f32[16,1,384]{2,1,0:T(1,128)S(1)}, u32[]{:S(2)}, u32[]{:S(2)}) %all-to-all-start) | async-done | bytes 24608 | tf_op jit(solution)/shard_map/all_to_all | solution.py:30
  76.8 0.1 multiply_convert_fusion
  76.9 2.9 %gather_fusion = bf16[1152,128]{1,0:T(8,128)(2,1)S(1)} fusion(bf16[385,128]{1,0:T(8,128)(2,1)S(1)} %concatenate.11, s32[2048]{0:T(1024)S(1)} %pad_clamp_fusion), kind=kCustom, calls=%fused_computation | custom fusion | bytes 594432 | tf_op jit(solution)/shard_map/gather | solution.py:129
  79.8 0.1 all_to_all.21
  79.9 24.5 %all_to_all.30 = bf16[32,36,128]{2,1,0:T(8,128)(2,1)S(1)} all-to-all(bf16[32,36,128]{2,1,0:T(8,128)(2,1)S(1)} %all_to_all.21), channel_id=1, replica_groups=mesh['sp'=32,'tp'=16] {'sp'}, dimensions={0} | all-to-all | bytes 589824 | tf_op jit(solution)/shard_map/all_to_all | solution.py:129
  104.4 0.8 all_to_all.23
  105.2 0.0 all-gather.8.cloned.1.call-start
  105.2 45.1 %all-gather.6.cloned.1.call-done = bf16[1152,2048]{1,0:T(8,128)(2,1)} async-done(((bf16[1152,128]{1,0:T(8,128)(2,1)}), bf16[1152,2048]{1,0:T(8,128)(2,1)}) %all-gather.6.cloned.1.call-update) | async-done | bytes 4718608 | tf_op jit(solution)/shard_map/all_gather | solution.py:130
  150.3 3.9 %fusion.7 = f32[1152,256]{1,0:T(8,128)S(1)} fusion(bf16[1152,2048]{1,0:T(8,128)(2,1)} %all-gather.6.cloned.1.call-done, bf16[1,2048,256]{2,1,0:T(8,128)(2,1)S(1)} %copy-done), kind=kOutput, calls=%fused_computation.14 | convolution fusion | flops 1207959552 | bytes 6946816 | tf_op jit(solution)/shard_map/dot_general | solution.py:133
  154.2 2.3 fusion
  156.7 71.4 %all-gather.8.cloned.1.call-done = bf16[1152,4096]{1,0:T(8,128)(2,1)} async-done(((bf16[1152,256]{1,0:T(8,128)(2,1)}), bf16[1152,4096]{1,0:T(8,128)(2,1)}) %all-gather.8.cloned.1.call-update) | async-done | bytes 9437200 | tf_op jit(solution)/shard_map/all_gather | solution.py:138
  228.1 6.5 %convolution_convert_fusion = bf16[1152,128]{1,0:T(8,128)(2,1)S(1)} fusion(bf16[1152,4096]{1,0:T(8,128)(2,1)} %all-gather.8.cloned.1.call-done, bf16[1,4096,128]{2,1,0:T(8,128)(2,1)} %param.25), kind=kOutput, calls=%fused_computation.5 | convolution fusion | flops 1208107008 | bytes 10780672 | tf_op jit(solution)/shard_map/dot_general | solution.py:137
  234.6 0.8 all_to_all.24
  235.3 9.0 %all-to-all-start.2 = ((bf16[32,36,128]{2,1,0:T(8,128)(2,1)}), bf16[32,36,128]{2,1,0:T(8,128)(2,1)S(1)}, u32[]{:S(2)}, u32[]{:S(2)}) async-start(bf16[32,36,128]{2,1,0:T(8,128)(2,1)} %all_to_all.24), calls=%async_computation.2 | async-start | bytes 655360 | tf_op jit(solution)/shard_map/all_to_all | solution.py:142
  244.4 0.1 copy.33
  244.6 14.4 %all-to-all-done.2 = bf16[32,36,128]{2,1,0:T(8,128)(2,1)S(1)} async-done(((bf16[32,36,128]{2,1,0:T(8,128)(2,1)}), bf16[32,36,128]{2,1,0:T(8,128)(2,1)S(1)}, u32[]{:S(2)}, u32[]{:S(2)}) %all-to-all-start.2) | async-done | bytes 294944 | tf_op jit(solution)/shard_map/all_to_all | solution.py:142
  259.0 0.1 all_to_all.26
  259.0 1.9 gather_fusion.1
  260.9 0.6 fusion.9
  261.5 0.7 add_convert_fusion
  (49 shorter events, 0.4 us)
Async XLA Ops:
  6.5 143.8 %copy-start = (bf16[1,2048,256]{2,1,0:T(8,128)(2,1)S(1)}, bf16[1,2048,256]{2,1,0:T(8,128)(2,1)}, u32[]{:S(2)}) copy-start(bf16[1,2048,256]{2,1,0:T(8,128)(2,1)} %param.23) | copy-start | bytes 3145732
  6.5 7.1 %copy-start.5 = (bf16[64,384]{1,0:T(8,128)(2,1)S(1)}, bf16[64,384]{1,0:T(8,128)(2,1)}, u32[]{:S(2)}) copy-start(bf16[64,384]{1,0:T(8,128)(2,1)} %param.14) | copy-start | bytes 147460
  6.5 7.8 %copy-start.8 = (s32[384,2]{0,1:T(2,128)S(1)}, s32[384,2]{0,1:T(2,128)}, u32[]{:S(2)}) copy-start(s32[384,2]{0,1:T(2,128)} %param.20) | copy-start | bytes 9220
  6.5 54.1 %all-gather.4.cloned.1.call-start = ((), (), s32[]{:S(2)}) async-start(), calls=%async_computation.3 | async-start | bytes 1671168 | tf_op jit(solution)/shard_map/all_gather | solution.py:25
  7.4 4.8 %collective-permute-start = (bf16[64,15]{1,0:T(8,128)(2,1)S(1)}, bf16[64,15]{1,0:T(8,128)(2,1)S(1)}, u32[]{:S(2)}, u32[]{:S(2)}) collective-permute-start(bf16[64,15]{1,0:T(8,128)(2,1)S(1)} %slice.43), channel_id=1, source_target_pairs={{0,16},{16,32},{32,48},{48,64},{64,80},{80,96},{96,112},{112,128},... | collective-permute-start | bytes 5768 | tf_op jit(solution)/shard_map/ppermute | solution.py:16
  14.4 46.3 %copy-start.2 = (bf16[4,256,256]{2,1,0:T(8,128)(2,1)S(1)}, bf16[4,256,256]{2,1,0:T(8,128)(2,1)}, u32[]{:S(2)}) copy-start(bf16[4,256,256]{2,1,0:T(8,128)(2,1)} %param.15) | copy-start | bytes 1572868
  60.6 1.6 slice-start
  60.7 2.1 copy-start.1
  60.7 2.1 copy-start.9
  62.8 1.0 copy-start.3
  62.8 1.0 copy-start.4
  62.8 13.9 %copy-start.10 = (f32[128]{0:T(128)S(1)}, f32[128]{0:T(128)}, u32[]{:S(2)}) copy-start(f32[128]{0:T(128)} %param.19) | copy-start | bytes 1540
  64.9 11.8 %all-to-all-start = ((f32[16,1,384]{2,1,0:T(1,128)}), f32[16,1,384]{2,1,0:T(1,128)S(1)}, u32[]{:S(2)}, u32[]{:S(2)}) async-start(f32[16,1,384]{2,1,0:T(1,128)} %broadcast_in_dim.69), calls=%async_computation | async-start | bytes 49152 | tf_op jit(solution)/shard_map/all_to_all | solution.py:30
  71.3 79.0 %all-gather.6.cloned.1.call-start = ((), (), s32[]{:S(2)}) async-start(), calls=%async_computation.4 | async-start | bytes 5013504 | tf_op jit(solution)/shard_map/all_gather | solution.py:130
  105.2 49.0 %copy-start.12 = (bf16[1,2048,256]{2,1,0:T(8,128)(2,1)S(1)}, bf16[1,2048,256]{2,1,0:T(8,128)(2,1)}, u32[]{:S(2)}) copy-start(bf16[1,2048,256]{2,1,0:T(8,128)(2,1)} %param.24) | copy-start | bytes 3145732
  105.2 122.9 %all-gather.8.cloned.1.call-start = ((), (), s32[]{:S(2)}) async-start(), calls=%async_computation.5 | async-start | bytes 10027008 | tf_op jit(solution)/shard_map/all_gather | solution.py:138
  150.3 3.9 %copy-start.11 = (bf16[1152,2048]{1,0:T(8,128)(2,1)S(1)}, bf16[1152,2048]{1,0:T(8,128)(2,1)}, u32[]{:S(2)}) copy-start(bf16[1152,2048]{1,0:T(8,128)(2,1)} %all-gather.6.cloned.1.call-done) | copy-start | bytes 14155780
  154.2 2.4 copy-start.6
  156.7 87.7 %copy-start.7 = (f32[384,2]{0,1:T(2,128)S(1)}, f32[384,2]{0,1:T(2,128)}, u32[]{:S(2)}) copy-start(f32[384,2]{0,1:T(2,128)} %param.22) | copy-start | bytes 9220
  235.3 23.6 %all-to-all-start.2 = ((bf16[32,36,128]{2,1,0:T(8,128)(2,1)}), bf16[32,36,128]{2,1,0:T(8,128)(2,1)S(1)}, u32[]{:S(2)}, u32[]{:S(2)}) async-start(bf16[32,36,128]{2,1,0:T(8,128)(2,1)} %all_to_all.24), calls=%async_computation.2 | async-start | bytes 655360 | tf_op jit(solution)/shard_map/all_to_all | solution.py:142
Sparse Core Ops, SparseCore 0:
  14.5 46.1 all-gather.3
  105.3 44.9 all-gather.5
  156.7 71.2 all-gather.7
where the time goes:
time: 269 us
  waiting for transfers between devices  178 us (66%)
  blocking collectives  24.5 us (9%)
  starting transfers between devices  18.8 us (7%)
  local copies, waits for them, and re-layouts  14.7 us (5%)
  matrix products  13.7 us (5%)
  between operations  13.5 us (5%)
  other arithmetic  5.95 us (2%)
    all_gather x1, waiting for transfers between devices, per_device(): lax.all_gather(activated, 'tp', axis=1, tiled=True)  71.4 us
    all_gather x1, waiting for transfers between devices, per_device(): portion = lax.all_gather(arrived, 'tp', axis=1, tiled=True)  45.1 us
    all_gather x1, waiting for transfers between devices, in_one_piece(): lax.all_gather(both, axis, axis=dim, tiled=True)  39.9 us
    all_to_all x1, blocking collectives, per_device(): lax.all_to_all(padded[sources], 'sp', split_axis=0, concat_axis=0, tiled=...  24.5 us
    all_to_all x1, waiting for transfers between devices, per_device(): lax.all_to_all(result, 'sp', split_axis=0, concat_axis=0, tiled=True)  14.4 us
    all_to_all x1, starting transfers between devices, per_device(): lax.all_to_all(result, 'sp', split_axis=0, concat_axis=0, tiled=True)  8.98 us
    dot_general x1, matrix products, per_device(): jnp.dot(lax.all_gather(activated, 'tp', axis=1, tiled=True), rows_down, p...  6.52 us
    all_to_all x1, starting transfers between devices, from_everyone(): lax.all_to_all(jnp.broadcast_to(value[None], (count, *value.shape)), axis...  6.36 us
  transfers between devices with their start and end apart: 6, of which 6 were waited for; matrix products, arithmetic and copies ran while one was open for 2% of the time, Pallas kernels for 0%

commit v1 on v0

--- a/solution.py
+++ b/solution.py
@@ -135,7 +135,9 @@
     activated = (jax.nn.silu(gate_term) * up_term).astype(jnp.bfloat16)
     rows_down = w_down[0]
     result = jnp.dot(
-        lax.all_gather(activated, "tp", axis=1, tiled=True),
+        jnp.concatenate(
+            lax.all_to_all(jnp.stack([activated] * lax.axis_size("tp")), "tp", 0, 0), axis=1
+        ),
         rows_down,
         preferred_element_type=jnp.float32,
     ).astype(jnp.bfloat16)

time: 269 us -> 415 us (1.54)
  the two profiles are of different devices: /device:TPU:16 before, /device:TPU:24 now
where the time goes in v1:
time: 415 us
  waiting for transfers between devices  313 us (75%)
  starting transfers between devices  25 us (6%)
  blocking collectives  24.5 us (6%)
  local copies, waits for them, and re-layouts  19.9 us (5%)
  between operations  13.8 us (3%)
  matrix products  12.8 us (3%)
  other arithmetic  5.95 us (1%)
    all_to_all x1, waiting for transfers between devices, per_device(): lax.all_to_all(jnp.stack([activated] * lax.axis_size('tp')), 'tp', 0, 0)  206 us
    all_gather x1, waiting for transfers between devices, per_device(): portion = lax.all_gather(arrived, 'tp', axis=1, tiled=True)  45.8 us
    all_gather x1, waiting for transfers between devices, in_one_piece(): lax.all_gather(both, axis, axis=dim, tiled=True)  41 us
    all_to_all x1, blocking collectives, per_device(): lax.all_to_all(padded[sources], 'sp', split_axis=0, concat_axis=0, tiled=...  24.5 us
    all_to_all x1, waiting for transfers between devices, per_device(): lax.all_to_all(result, 'sp', split_axis=0, concat_axis=0, tiled=True)  14.2 us
    all_to_all x1, starting transfers between devices, per_device(): lax.all_to_all(result, 'sp', split_axis=0, concat_axis=0, tiled=True)  9.07 us
  transfers between devices with their start and end apart: 6, of which 6 were waited for; matrix products, arithmetic and copies ran while one was open for 2% of the time, Pallas kernels for 0%

profile of v1, /device:TPU:24, one launch (start us, length us, event | category | flops | bytes accessed | tf_op | source)
XLA Modules:
  0.0 414.9 jit_solution(18234477456770079069)
XLA Ops:
  6.5 0.9 slice.43
  7.4 3.4 collective-permute-start
  10.9 1.3 collective-permute-done
  12.2 0.9 maximum_convert_fusion
  13.1 0.1 slice_add_fusion.2
  13.2 0.1 slice_add_fusion.1
  13.3 0.1 slice_add_fusion
  13.5 0.2 fusion.13
  13.7 0.7 pad_maximum_fusion
  14.4 0.1 copy.38
  14.5 0.1 eq.69
  14.7 0.1 eq.65
  14.8 1.7 reduce-window.6
  16.6 0.3 slice_reduce_fusion
  16.9 0.1 copy.37
  17.0 0.2 mul.134
  17.2 0.1 fusion.12
  17.3 3.4 scatter_custom_fusion
  20.7 41.0 %all-gather.3.cloned.1.call-done = bf16[1024,768]{1,0:T(8,128)(2,1)} async-done(((bf16[64,768]{1,0:T(8,128)(2,1)}), bf16[1024,768]{1,0:T(8,128)(2,1)}) %all-gather.3.cloned.1.call-update) | async-done | bytes 1572880 | tf_op jit(solution)/shard_map/all_gather | solution.py:25
  61.8 1.6 slice-done
  63.4 0.5 fusion.26
  64.0 0.4 fusion.2
  64.4 0.5 copy-done.3
  64.9 0.5 multiply_reduce_fusion
  65.4 0.6 broadcast_in_dim.69
  66.0 5.1 %all-to-all-start = ((f32[16,1,384]{2,1,0:T(1,128)}), f32[16,1,384]{2,1,0:T(1,128)S(1)}, u32[]{:S(2)}, u32[]{:S(2)}) async-start(f32[16,1,384]{2,1,0:T(1,128)} %broadcast_in_dim.69), calls=%async_computation | async-start | bytes 49152 | tf_op jit(solution)/shard_map/all_to_all | solution.py:30
  71.2 4.5 %all-to-all-done = f32[16,1,384]{2,1,0:T(1,128)S(1)} async-done(((f32[16,1,384]{2,1,0:T(1,128)}), f32[16,1,384]{2,1,0:T(1,128)S(1)}, u32[]{:S(2)}, u32[]{:S(2)}) %all-to-all-start) | async-done | bytes 24608 | tf_op jit(solution)/shard_map/all_to_all | solution.py:30
  75.8 0.1 multiply_convert_fusion
  75.9 2.9 gather_fusion
  78.8 0.1 all_to_all.24
  78.9 24.5 %all_to_all.35 = bf16[32,36,128]{2,1,0:T(8,128)(2,1)S(1)} all-to-all(bf16[32,36,128]{2,1,0:T(8,128)(2,1)S(1)} %all_to_all.24), channel_id=1, replica_groups=mesh['sp'=32,'tp'=16] {'sp'}, dimensions={0} | all-to-all | bytes 589824 | tf_op jit(solution)/shard_map/all_to_all | solution.py:129
  103.4 0.8 all_to_all.26
  104.2 45.8 %all-gather.5.cloned.1.call-done = bf16[1152,2048]{1,0:T(8,128)(2,1)} async-done(((bf16[1152,128]{1,0:T(8,128)(2,1)}), bf16[1152,2048]{1,0:T(8,128)(2,1)}) %all-gather.5.cloned.1.call-update) | async-done | bytes 4718608 | tf_op jit(solution)/shard_map/all_gather | solution.py:130
  150.0 3.9 fusion.7
  153.9 1.5 fusion
  155.5 0.3 copy.41
  155.8 4.9 %stack.2 = bf16[16,1152,256]{1,2,0:T(8,128)(2,1)} broadcast(bf16[1152,256]{0,1:T(8,128)(2,1)S(1)} %copy.41), dimensions={1,2} | broadcast | bytes 10027008 | tf_op jit(solution)/shard_map/stack | solution.py:139
  160.7 7.4 %all-to-all-start.2 = ((bf16[16,1152,256]{1,2,0:T(8,128)(2,1)}), bf16[16,1152,256]{1,2,0:T(8,128)(2,1)}, u32[]{:S(2)}, u32[]{:S(2)}) async-start(bf16[16,1152,256]{1,2,0:T(8,128)(2,1)} %stack.2), calls=%async_computation.2 | async-start | bytes 18874368 | tf_op jit(solution)/shard_map/all_to_all | solution.py:139
  168.1 206.1 %all-to-all-done.2 = bf16[16,1152,256]{1,2,0:T(8,128)(2,1)} async-done(((bf16[16,1152,256]{1,2,0:T(8,128)(2,1)}), bf16[16,1152,256]{1,2,0:T(8,128)(2,1)}, u32[]{:S(2)}, u32[]{:S(2)}) %all-to-all-start.2) | async-done | bytes 9437216 | tf_op jit(solution)/shard_map/all_to_all | solution.py:139
  374.2 6.4 %convolution_convert_fusion = bf16[1152,128]{1,0:T(8,128)(2,1)S(1)} fusion(bf16[1152,4096]{0,1:T(8,128)(2,1)} %bitcast.8, bf16[1,4096,128]{2,1,0:T(8,128)(2,1)S(1)} %copy-done.13), kind=kOutput, calls=%fused_computation.5 | convolution fusion | flops 1208107008 | bytes 10780672 | tf_op jit(solution)/shard_map/dot_general | solution.py:137
  380.5 0.8 all_to_all.28
  381.3 9.1 %all-to-all-start.3 = ((bf16[32,36,128]{2,1,0:T(8,128)(2,1)}), bf16[32,36,128]{2,1,0:T(8,128)(2,1)S(1)}, u32[]{:S(2)}, u32[]{:S(2)}) async-start(bf16[32,36,128]{2,1,0:T(8,128)(2,1)} %all_to_all.28), calls=%async_computation.3 | async-start | bytes 655360 | tf_op jit(solution)/shard_map/all_to_all | solution.py:144
  390.5 0.1 copy.35
  390.6 14.2 %all-to-all-done.3 = bf16[32,36,128]{2,1,0:T(8,128)(2,1)S(1)} async-done(((bf16[32,36,128]{2,1,0:T(8,128)(2,1)}), bf16[32,36,128]{2,1,0:T(8,128)(2,1)S(1)}, u32[]{:S(2)}, u32[]{:S(2)}) %all-to-all-start.3) | async-done | bytes 294944 | tf_op jit(solution)/shard_map/all_to_all | solution.py:144
  404.9 0.1 all_to_all.30
  404.9 1.9 gather_fusion.1
  406.8 0.6 fusion.9
  407.4 0.7 add_convert_fusion
  (52 shorter events, 0.4 us)
Async XLA Ops:
  6.5 143.5 %copy-start = (bf16[1,2048,256]{2,1,0:T(8,128)(2,1)S(1)}, bf16[1,2048,256]{2,1,0:T(8,128)(2,1)}, u32[]{:S(2)}) copy-start(bf16[1,2048,256]{2,1,0:T(8,128)(2,1)} %param.23) | copy-start | bytes 3145732
  6.5 7.1 %copy-start.5 = (bf16[64,384]{1,0:T(8,128)(2,1)S(1)}, bf16[64,384]{1,0:T(8,128)(2,1)}, u32[]{:S(2)}) copy-start(bf16[64,384]{1,0:T(8,128)(2,1)} %param.14) | copy-start | bytes 147460
  6.5 7.8 %copy-start.8 = (s32[384,2]{0,1:T(2,128)S(1)}, s32[384,2]{0,1:T(2,128)}, u32[]{:S(2)}) copy-start(s32[384,2]{0,1:T(2,128)} %param.20) | copy-start | bytes 9220
  6.5 55.2 %all-gather.3.cloned.1.call-start = ((), (), s32[]{:S(2)}) async-start(), calls=%async_computation.4 | async-start | bytes 1671168 | tf_op jit(solution)/shard_map/all_gather | solution.py:25
  7.4 4.8 %collective-permute-start = (bf16[64,15]{1,0:T(8,128)(2,1)S(1)}, bf16[64,15]{1,0:T(8,128)(2,1)S(1)}, u32[]{:S(2)}, u32[]{:S(2)}) collective-permute-start(bf16[64,15]{1,0:T(8,128)(2,1)S(1)} %slice.43), channel_id=1, source_target_pairs={{0,16},{16,32},{32,48},{48,64},{64,80},{80,96},{96,112},{112,128},... | collective-permute-start | bytes 5768 | tf_op jit(solution)/shard_map/ppermute | solution.py:16
  14.4 47.4 %copy-start.2 = (bf16[4,256,256]{2,1,0:T(8,128)(2,1)S(1)}, bf16[4,256,256]{2,1,0:T(8,128)(2,1)}, u32[]{:S(2)}) copy-start(bf16[4,256,256]{2,1,0:T(8,128)(2,1)} %param.15) | copy-start | bytes 1572868
  61.8 1.6 slice-start
  61.8 2.1 copy-start.1
  61.8 2.1 copy-start.9
  63.9 1.0 copy-start.3
  63.9 1.0 copy-start.4
  64.0 11.8 %copy-start.10 = (f32[128]{0:T(128)S(1)}, f32[128]{0:T(128)}, u32[]{:S(2)}) copy-start(f32[128]{0:T(128)} %param.19) | copy-start | bytes 1540
  66.0 9.7 %all-to-all-start = ((f32[16,1,384]{2,1,0:T(1,128)}), f32[16,1,384]{2,1,0:T(1,128)S(1)}, u32[]{:S(2)}, u32[]{:S(2)}) async-start(f32[16,1,384]{2,1,0:T(1,128)} %broadcast_in_dim.69), calls=%async_computation | async-start | bytes 49152 | tf_op jit(solution)/shard_map/all_to_all | solution.py:30
  71.1 78.9 %all-gather.5.cloned.1.call-start = ((), (), s32[]{:S(2)}) async-start(), calls=%async_computation.5 | async-start | bytes 5013504 | tf_op jit(solution)/shard_map/all_gather | solution.py:130
  104.2 49.8 %copy-start.12 = (bf16[1,2048,256]{2,1,0:T(8,128)(2,1)S(1)}, bf16[1,2048,256]{2,1,0:T(8,128)(2,1)}, u32[]{:S(2)}) copy-start(bf16[1,2048,256]{2,1,0:T(8,128)(2,1)} %param.24) | copy-start | bytes 3145732
  150.0 3.9 copy-start.11
  160.7 7.4 %copy-start.6 = (f32[384,4]{0,1:T(4,128)S(1)}, f32[384,4]{0,1:T(4,128)}, u32[]{:S(2)}) copy-start(f32[384,4]{0,1:T(4,128)} %param.21) | copy-start | bytes 18436
  160.7 213.5 %copy-start.13 = (bf16[1,4096,128]{2,1,0:T(8,128)(2,1)S(1)}, bf16[1,4096,128]{2,1,0:T(8,128)(2,1)}, u32[]{:S(2)}) copy-start(bf16[1,4096,128]{2,1,0:T(8,128)(2,1)} %param.25) | copy-start | bytes 3145732
  160.7 213.5 %all-to-all-start.2 = ((bf16[16,1152,256]{1,2,0:T(8,128)(2,1)}), bf16[16,1152,256]{1,2,0:T(8,128)(2,1)}, u32[]{:S(2)}, u32[]{:S(2)}) async-start(bf16[16,1152,256]{1,2,0:T(8,128)(2,1)} %stack.2), calls=%async_computation.2 | async-start | bytes 18874368 | tf_op jit(solution)/shard_map/all_to_all | solution.py:139
  374.2 16.2 %copy-start.7 = (f32[384,2]{0,1:T(2,128)S(1)}, f32[384,2]{0,1:T(2,128)}, u32[]{:S(2)}) copy-start(f32[384,2]{0,1:T(2,128)} %param.22) | copy-start | bytes 9220
  381.3 23.6 %all-to-all-start.3 = ((bf16[32,36,128]{2,1,0:T(8,128)(2,1)}), bf16[32,36,128]{2,1,0:T(8,128)(2,1)S(1)}, u32[]{:S(2)}, u32[]{:S(2)}) async-start(bf16[32,36,128]{2,1,0:T(8,128)(2,1)} %all_to_all.28), calls=%async_computation.3 | async-start | bytes 655360 | tf_op jit(solution)/shard_map/all_to_all | solution.py:144
Sparse Core Ops, SparseCore 0:
  14.5 47.2 all-gather.2
  104.3 45.6 all-gather.4
